TPU v7x, 32 devices: a whole 2x2x4 slice. The times are simulated.
32 devices in a mesh: sp: 8 (over z, x), tp: 4 (over y, core).
Axes of the slice: x: 2, y: 2, z: 4, core: 2. Of those that a mesh axis runs over, the one named last changes fastest.
Arguments:
- queries_one: bfloat16 [1024, 2048], P('sp', 'tp'), may hold values from -6.2 to 6.2
- keys_one: bfloat16 [1024, 2048], P('sp', 'tp'), may hold values from -5 to 5
- values_one: bfloat16 [1024, 2048], P('sp', 'tp'), may hold values from -6 to 6
- queries_two: bfloat16 [1024, 1024], P('sp', 'tp'), may hold values from -6.2 to 6.2
- keys_two: bfloat16 [1024, 1024], P('sp', 'tp'), may hold values from -5 to 5
- values_two: bfloat16 [1024, 1024], P('sp', 'tp'), may hold values from -6 to 6
- key_offset: bfloat16 [1024, 2, 16], P('sp', None, 'tp'), may hold values from -14 to 0
- out_one: bfloat16 [2048, 4096], P('tp'), may hold values from -0.109375 to 0.109375
- out_two: bfloat16 [1024, 4096], P('tp'), may hold values from -0.109375 to 0.109375
- residual: bfloat16 [1024, 4096], P('sp', 'tp'), may hold values from -6 to 6
- norm_gain: float32 [4096], replicated, may hold values from 0.1 to 1.9
- routes: int32 [1024, 2], P('sp'), may hold values from 0 to 7, all different within a row; in each aligned block of 128 rows (0 to 127, 128 to 255, ...) at most 64 rows name the same one
- route_weight: float32 [1024, 2], P('sp'), may hold values from 0.2 to 1
- expert_gate: bfloat16 [8, 4096, 2048], P('sp', None, 'tp'), may hold values from -0.09375 to 0.09375
- expert_up: bfloat16 [8, 4096, 2048], P('sp', None, 'tp'), may hold values from -0.09375 to 0.09375
- expert_down: bfloat16 [8, 2048, 4096], P('sp', None, 'tp'), may hold values from -0.125 to 0.125
Outputs:
- mixed: bfloat16 [1024, 4096], P('sp', 'tp')
Inputs may be any that keep to these rules, and one draw needn't show every extreme that they name: `routes`: each row names two different experts; in each aligned block of 128 rows no expert is named more than 64 times, a bound that some block reaches.
All inputs are finite; a program needn't handle non-finite values.
Results may differ from a plain program's by a relative error of at most 0.015.
Values may be sent and summed in bfloat16 or wider, within the bound.
A program may use at most 64 MiB of HBM per device.

v0:
```python
import functools

import jax
import jax.numpy as jnp
from jax import lax
from jax.experimental import pallas as pl
from jax.experimental.pallas import tpu as pltpu
from jax.sharding import PartitionSpec as P

DH1 = 128
DH2 = 64


EPS = 1e-06


def stick_group(query, keys, values, offset, head_size, own_start, key_block):
    row_count = query.shape[0]
    head_count = query.shape[1] // head_size
    query_heads = query.reshape(row_count, head_count, head_size)
    query_pos = own_start + jnp.arange(row_count, dtype=jnp.int32)
    block_count = (own_start + row_count + key_block - 1) // key_block

    def key_step(step_index, state_pair):
        summed, carried = state_pair
        first_key = (block_count - 1 - step_index) * key_block
        key_rows = lax.dynamic_slice_in_dim(keys, first_key, key_block, 0).reshape(
            key_block, head_count, head_size
        )
        value_rows = lax.dynamic_slice_in_dim(values, first_key, key_block, 0).reshape(
            key_block, head_count, head_size
        )
        bias_rows = lax.dynamic_slice_in_dim(offset, first_key, key_block, 0).astype(jnp.float32)
        scores = jnp.einsum(
            "qhd,khd->hqk", query_heads, key_rows, preferred_element_type=jnp.float32
        )
        scores = scores * head_size ** (-0.5) + bias_rows.T[:, None, :]
        key_pos = first_key + jnp.arange(key_block, dtype=jnp.int32)
        causal = key_pos[None, :] < query_pos[:, None]
        log_beta = jax.nn.log_sigmoid(scores)
        log_rest = jnp.where(causal, jax.nn.log_sigmoid(-scores), 0.0)
        shifted = jnp.pad(log_rest[..., 1:], ((0, 0), (0, 0), (0, 1)))
        within = lax.cumsum(shifted, axis=2, reverse=True)
        weights = jnp.where(causal, jnp.exp(log_beta + within + carried[..., None]), 0.0).astype(
            jnp.bfloat16
        )
        summed = summed + jnp.einsum(
            "hqk,khd->hqd", weights, value_rows, preferred_element_type=jnp.float32
        )
        carried = carried + jnp.sum(log_rest, axis=2)
        return (summed, carried)

    start_state = (
        jnp.zeros((head_count, row_count, head_size), jnp.float32),
        jnp.zeros((head_count, row_count), jnp.float32),
    )
    summed, _ = lax.fori_loop(0, block_count, key_step, start_state)
    return summed.transpose(1, 0, 2).reshape(row_count, head_count * head_size).astype(jnp.bfloat16)


def body(
    queries_one,
    keys_one,
    values_one,
    queries_two,
    keys_two,
    values_two,
    key_offset,
    out_one,
    out_two,
    residual,
    norm_gain,
    routes,
    route_weight,
    expert_gate,
    expert_up,
    expert_down,
):
    row_count = queries_one.shape[0]
    spread = lax.axis_size("sp")
    tp_count = lax.axis_size("tp")
    own_start = lax.axis_index("sp") * row_count
    factor = max(1, min(spread, 512 // row_count))
    while spread % factor:
        factor -= 1
    key_block = row_count * factor
    far_k1, far_v1, far_k2, far_v2, far_offset = (
        lax.all_gather(keys_one, "sp", axis=0, tiled=True),
        lax.all_gather(values_one, "sp", axis=0, tiled=True),
        lax.all_gather(keys_two, "sp", axis=0, tiled=True),
        lax.all_gather(values_two, "sp", axis=0, tiled=True),
        lax.all_gather(key_offset, "sp", axis=0, tiled=True),
    )
    attended_one = stick_group(
        queries_one, far_k1, far_v1, far_offset[:, 0, :], DH1, own_start, key_block
    )
    attended_two = stick_group(
        queries_two, far_k2, far_v2, far_offset[:, 1, :], DH2, own_start, key_block
    )
    partial_value = jnp.dot(attended_one, out_one, preferred_element_type=jnp.float32)
    partial_value = partial_value + jnp.dot(
        attended_two, out_two, preferred_element_type=jnp.float32
    )
    columns = residual.shape[1]
    column_start = lax.axis_index("tp") * columns
    resid_full = lax.all_gather(residual, "tp", axis=1, tiled=True)
    projected = lax.psum(partial_value.astype(jnp.bfloat16), "tp").astype(jnp.float32)
    stream = (resid_full.astype(jnp.float32) + projected).astype(jnp.bfloat16)
    stream_f = stream.astype(jnp.float32)
    normed = (
        stream_f * lax.rsqrt(jnp.mean(stream_f * stream_f, axis=1, keepdims=True) + EPS) * norm_gain
    ).astype(jnp.bfloat16)
    stream_own = lax.dynamic_slice_in_dim(stream, column_start, columns, 1)
    capacity = tp_count * ((4 * row_count // spread + tp_count - 1) // tp_count)
    flat_ids = routes.reshape(-1)
    onehot = (flat_ids[:, None] == jnp.arange(spread, dtype=jnp.int32)[None, :]).astype(jnp.int32)
    before = jnp.cumsum(onehot, axis=0) - onehot
    slot_of = flat_ids * capacity + jnp.sum(before * onehot, axis=1)
    chosen = slot_of[:, None] == jnp.arange(spread * capacity, dtype=jnp.int32)[None, :]
    selector = jnp.any(chosen.reshape(row_count, 2, spread * capacity), axis=1).T.astype(
        jnp.bfloat16
    )
    outgoing = jnp.dot(selector, normed, preferred_element_type=jnp.float32).astype(jnp.bfloat16)
    outgoing = outgoing.reshape(spread, capacity, normed.shape[1])
    gate_w = expert_gate[0]
    up_w = expert_up[0]
    down_w = expert_down[0]
    share_size = capacity // tp_count
    own_part = lax.dynamic_slice_in_dim(outgoing, lax.axis_index("tp") * share_size, share_size, 1)
    arrived = lax.all_to_all(own_part, "sp", split_axis=0, concat_axis=0, tiled=True)
    arrived = lax.all_gather(arrived, "tp", axis=1, tiled=True)
    sources, items, _ = arrived.shape
    flat_rows = arrived.reshape(sources * items, arrived.shape[2])
    gate_act = jnp.dot(flat_rows, gate_w, preferred_element_type=jnp.float32)
    up_act = jnp.dot(flat_rows, up_w, preferred_element_type=jnp.float32)
    hidden = (jax.nn.silu(gate_act) * up_act).astype(jnp.bfloat16)
    summed = jnp.dot(
        lax.all_gather(hidden, "tp", axis=1, tiled=True), down_w, preferred_element_type=jnp.float32
    )
    returned = lax.all_to_all(
        summed.astype(jnp.bfloat16).reshape(sources, items, down_w.shape[1]),
        "sp",
        split_axis=0,
        concat_axis=0,
        tiled=True,
    )
    back_rows = returned.reshape(spread * capacity, returned.shape[2])
    picked = jnp.dot(chosen.astype(jnp.bfloat16), back_rows, preferred_element_type=jnp.float32)
    picked = picked.reshape(row_count, 2, back_rows.shape[1])
    combined = route_weight[:, 0:1] * picked[:, 0] + route_weight[:, 1:2] * picked[:, 1]
    return (stream_own.astype(jnp.float32) + combined).astype(jnp.bfloat16)


BF = jnp.bfloat16
F32 = jnp.float32


def to(sp, tp):
    return {"device_id": (sp, tp), "device_id_type": pl.DeviceIdType.MESH}


def is_wide(index):
    return (index // 2 + index) % 2 == 0


def flipped(index, mask, n):
    place, total = 1, 0
    while place < n:
        bit = index // place % 2
        total = total + place * (1 - bit if mask & place else bit)
        place *= 2
    return total


def turns(n):
    near = list(range(n // 2))
    far = list(range(n - n // 4, n)) + list(range(n // 2, n - n // 4))
    listed, rest = near[:2], near[2:]
    for mask in far:
        listed.append(mask)
        if rest:
            listed.append(rest.pop(0))
    return listed + rest


def neighbours(tp, t):
    partner = tp + 1 - 2 * (tp % 2)
    across = (tp + 2) % t
    return partner, across, across + 1 - 2 * (across % 2)


def layer_kernel(
    n, t, h1, h2, cap,
    off_in, routes, route_weight,
    q1_hbm, k1_hbm, v1_hbm, q2_hbm, k2_hbm, v2_hbm, w1_hbm, w2_hbm, resid_hbm,
    gate_hbm, up_hbm, down_hbm, gain_hbm,
    out,
    q1_in, k1_in, v1_in, q2_in, k2_in, v2_in, w1_in, w2_in, resid_in, gate_in, up_in, down_in, gain,
    pk, buf, off, offbuf, carry, acc, obuf, att,
    pair_out, pair_in, far_out, far_in, stat_out, stat_in, stream_keep, chosen, weights,
    sbuf, xbuf, hbuf, rbuf, backbuf,
    wsem, qs, qr, fs, fr, os_, or_, ps, pr, ys, yr, ss, sr,
    ds_, dr, xs, xr, hs, hr, rs, rr,
):
    in_hbm = (
        q1_hbm, k1_hbm, v1_hbm, q2_hbm, k2_hbm, v2_hbm, w1_hbm, w2_hbm, resid_hbm,
        gate_hbm, up_hbm, down_hbm,
    )
    in_vmem = (
        q1_in, k1_in, v1_in, q2_in, k2_in, v2_in, w1_in, w2_in, resid_in,
        gate_in, up_in, down_in,
    )
    me = lax.axis_index("sp")
    tp = lax.axis_index("tp")
    partner, across, diagonal = neighbours(tp, t)
    rows, cols = resid_in.shape
    peers = [(lax.rem(me + d, n), tp) for d in range(1, n)]
    peers += [(me, peer) for peer in (partner, across, diagonal)]
    barrier = pltpu.get_barrier_semaphore()
    for peer in peers:
        pl.semaphore_signal(barrier, inc=1, **to(*peer))
    own_gain = gain_hbm.at[:, pl.ds(pl.multiple_of(tp * cols, 128), cols)]
    pairs = list(zip(in_hbm, in_vmem)) + [(own_gain, gain)]
    loads = [pltpu.make_async_copy(a, b, wsem.at[i]) for i, (a, b) in enumerate(pairs)]
    for load in loads:
        load.start()
    q1, k1, v1, q2, k2, v2, w1, w2, resid_, gate, up, down = in_vmem
    for load in loads[:6]:
        load.wait()
    for g in range(2):
        for h in range(off_in.shape[1]):
            off[2 * h + (h + g) % 2] = jnp.broadcast_to(off_in[g, h : h + 1, :].astype(F32), (8, rows))
    for h in range(h2):
        lanes = slice(h * DH2, (h + 1) * DH2)
        pk[h, 0] = jnp.concatenate([q2[:, lanes], k2[:, lanes]], axis=1)
        pk[h, 1] = jnp.concatenate([v2[:, lanes], jnp.zeros((rows, DH1 - DH2), BF)], axis=1)
    pl.semaphore_wait(barrier, len(peers))

    def wide(dest, origin, d, part):
        src = (q1, k1, v1)[part]
        return pltpu.make_async_remote_copy(
            src.at[:, pl.ds(pl.multiple_of(dest // 2 * DH1, DH1), DH1)],
            buf.at[part, origin], qs.at[d, part], qr.at[d, part], **to(dest, tp),
        )

    def narrow(dest, origin, d, part):
        return pltpu.make_async_remote_copy(
            pk.at[dest // 2, part // 2],
            buf.at[part, origin], qs.at[d, part], qr.at[d, part], **to(dest, tp),
        )

    def offs(dest, d):
        return pltpu.make_async_remote_copy(
            off.at[dest], offbuf.at[me], fs.at[d], fr.at[d], **to(dest, tp)
        )

    order = [d for pair in zip(range(n // 2, n), range(n // 2 - 1, -1, -1)) for d in pair if d]
    for d in order:
        dest = lax.rem(me + d, n)

        @pl.when(is_wide(dest))
        def _():
            for part in (0, 1, 2):
                wide(dest, me, d, part).start()

        @pl.when(jnp.logical_not(is_wide(dest)))
        def _():
            for part in (0, 2):
                narrow(dest, me, d, part).start()

        offs(dest, d).start()
    offbuf[me] = off[me]

    @pl.when(is_wide(me))
    def _():
        lanes = pl.ds(pl.multiple_of(me // 2 * DH1, DH1), DH1)
        buf[0, me] = q1[:, lanes]
        buf[1, me] = k1[:, lanes]
        buf[2, me] = v1[:, lanes]

    @pl.when(jnp.logical_not(is_wide(me)))
    def _():
        mine = me // 2
        buf[0, me] = pk[mine, 0]
        buf[2, me] = pk[mine, 1]

    table = jnp.concatenate(
        [routes[...].astype(F32), route_weight[...], jnp.zeros((128 - 4, rows), F32)], axis=0
    ).T
    lane = lax.broadcasted_iota(jnp.int32, (rows, 128), 1)
    row = lax.broadcasted_iota(jnp.int32, (rows, 128), 0)
    named = [table[:, k : k + 1] == lane.astype(F32) for k in (0, 1)]
    either = jnp.where(named[0] | named[1], 1.0, 0.0).astype(BF)
    earlier = jnp.where(lane < row, 1.0, 0.0).astype(BF)
    before = jnp.dot(earlier, either, preferred_element_type=F32)
    slots = lax.broadcasted_iota(jnp.int32, (rows, n * cap), 1).astype(F32)
    for k in (0, 1):
        slot = table[:, k : k + 1] * cap + jnp.sum(
            jnp.where(named[k], before, 0.0), axis=1, keepdims=True
        )
        chosen[k] = jnp.where(slots == slot, 1.0, 0.0).astype(BF)
        weights[k] = jnp.broadcast_to(table[:, 2 + k : 3 + k], (rows, 128))

    lane = lax.broadcasted_iota(jnp.int32, (DH1, 2 * DH1), 1)
    row = lax.broadcasted_iota(jnp.int32, (DH1, 2 * DH1), 0)
    tri = jnp.where((row > lane) | (lane >= DH1), 1.0, 0.0).astype(BF)
    scale = jnp.where(is_wide(me), DH1 ** -0.5, DH2 ** -0.5).astype(F32)
    nt = (((1,), (1,)), ((), ()))

    def block(i, j, own):
        s = lax.dot_general(buf[0, i], buf[1, j], nt, preferred_element_type=F32)
        s = s * scale + offbuf[j][0:1, :]
        soft = jnp.log(1.0 + jnp.exp(-jnp.abs(s)))
        log_beta = jnp.minimum(s, 0.0) - soft
        log_rest = log_beta - s
        if own:
            r = lax.broadcasted_iota(jnp.int32, s.shape, 0)
            c = lax.broadcasted_iota(jnp.int32, s.shape, 1)
            log_rest = jnp.where(c < r, log_rest, 0.0)
        high = log_rest.astype(BF)
        low = (log_rest - high.astype(F32)).astype(BF)
        sums = jnp.dot(high, tri, preferred_element_type=F32) + jnp.dot(
            low, tri, preferred_element_type=F32
        )
        weight = jnp.exp(log_beta + sums[:, :DH1])
        if own:
            weight = jnp.where(c < r, weight, 0.0)
        acc[i, j] = jnp.dot(weight.astype(BF), buf[2, j], preferred_element_type=F32)
        carry[i, j] = sums[:, DH1:]

    here = []
    for d in [0] + order:
        source = lax.rem(me + n - d, n)
        if d:
            dest = lax.rem(me + d, n)

            @pl.when(is_wide(me))
            def _():
                for part in (0, 1, 2):
                    wide(dest, me, d, part).wait_recv()

            @pl.when(jnp.logical_not(is_wide(me)))
            def _():
                for part in (0, 2):
                    narrow(dest, me, d, part).wait_recv()

            offs(dest, d).wait_recv()

        @pl.when(jnp.logical_not(is_wide(me)))
        def _():
            both = buf[0, source]
            zero = jnp.zeros((rows, DH1 - DH2), BF)
            buf[1, source] = jnp.concatenate([both[:, DH2:], zero], axis=1)
            buf[0, source] = jnp.concatenate([both[:, :DH2], zero], axis=1)

        block(source, source, True)
        for other in here:
            block(jnp.maximum(source, other), jnp.minimum(source, other), False)
        here.append(source)
    for i in range(n):
        total = acc[i, i]
        passed = carry[i, i]
        for j in range(i - 1, -1, -1):
            total = total + jnp.exp(passed) * acc[i, j]
            passed = passed + carry[i, j]
        obuf[i] = total.astype(BF)

    def back(dest, d):
        return pltpu.make_async_remote_copy(
            obuf.at[dest], att.at[me], os_.at[d], or_.at[d], **to(dest, tp)
        )

    for d in order:
        back(lax.rem(me + d, n), d).start()
    att[me] = obuf[me]
    for load in loads[6:9] + loads[12:]:
        load.wait()
    for d in range(1, n):
        back(lax.rem(me + d, n), d).wait_recv()

    a1 = jnp.concatenate([att[2 * h + h % 2] for h in range(h1)], axis=1)
    a2 = jnp.concatenate([att[2 * h + 1 - h % 2][:, :DH2] for h in range(h2)], axis=1)

    def partial(target):
        lanes = pl.ds(pl.multiple_of(target * cols, 128), cols)
        return jnp.dot(a1, w1[:, lanes], preferred_element_type=F32) + jnp.dot(
            a2, w2[:, lanes], preferred_element_type=F32
        )

    def pair(slot):
        return pltpu.make_async_remote_copy(
            pair_out.at[slot], pair_in.at[slot], ps.at[slot], pr.at[slot], **to(me, partner)
        )

    far = pltpu.make_async_remote_copy(far_out, far_in, ys.at[0], yr.at[0], **to(me, across))
    pair_out[0] = partial(diagonal).astype(BF)
    pair(0).start()
    there = partial(across)
    pair(0).wait_recv()
    far_out[...] = (there + pair_in[0].astype(F32)).astype(BF)
    far.start()
    pair_out[1] = partial(partner).astype(BF)
    pair(1).start()
    here = partial(tp)
    pair(1).wait_recv()
    here = here + pair_in[1].astype(F32)
    far.wait_recv()
    stream = (resid_[...].astype(F32) + (here + far_in[...].astype(F32))).astype(BF)
    stream_keep[...] = stream
    stream = stream.astype(F32)
    squares = jnp.sum(stream * stream, axis=1, keepdims=True)
    stat_out[0] = jnp.broadcast_to(squares, (rows, 128)).T[0:8, :]

    def stat(slot, peer):
        return pltpu.make_async_remote_copy(
            stat_out.at[0], stat_in.at[slot], ss.at[slot], sr.at[slot], **to(me, peer)
        )

    for slot, peer in enumerate((partner, across, diagonal)):
        stat(slot, peer).start()
    for slot, peer in enumerate((partner, across, diagonal)):
        stat(slot, peer).wait_recv()
    total = stat_out[0] + stat_in[0] + stat_in[1] + stat_in[2]
    total = jnp.broadcast_to(total[0:1, :], (128, rows)).T[:, 0:1]
    normed = (stream * lax.rsqrt(total / (t * cols) + EPS) * gain[...]).astype(BF)

    outgoing = lax.dot_general(
        chosen[0] + chosen[1], normed, (((0,), (0,)), ((), ())), preferred_element_type=F32
    ).astype(BF)
    for s in range(n):
        sbuf[s] = outgoing[s * cap : (s + 1) * cap]

    def send(d):
        dest = flipped(me, d, n)
        return pltpu.make_async_remote_copy(
            sbuf.at[dest], xbuf.at[tp, me], ds_.at[d], dr.at[d], **to(dest, tp)
        )

    def spread(ref, sends, recvs, kind, d):
        s = flipped(me, d, n)
        share = across if kind == 2 else tp
        peer = across if kind == 1 else partner
        return pltpu.make_async_remote_copy(
            ref.at[share, s], ref.at[share, s], sends.at[kind, d], recvs.at[kind, d],
            **to(me, peer),
        )

    x_move = functools.partial(spread, xbuf, xs, xr)
    h_move = functools.partial(spread, hbuf, hs, hr)

    def give(d):
        dest = flipped(me, d, n)
        return pltpu.make_async_remote_copy(
            rbuf.at[dest], backbuf.at[me], rs.at[d], rr.at[d], **to(dest, tp)
        )

    listed = turns(n)
    for d in listed[1:]:
        send(d).start()
    xbuf[tp, me] = sbuf[me]
    x_move(1, 0).start()
    x_move(0, 0).start()
    for load in loads[9:12]:
        load.wait()

    def forward(d):
        send(d).wait_recv()
        x_move(1, d).start()
        x_move(0, d).start()

    def relay(move, d):
        move(1, d).wait_recv()
        move(2, d).start()

    def settle(move, d):
        move(0, d).wait_recv()
        move(2, d).wait_recv()

    groups = n // 2

    for g in range(groups + 2):
        if g < groups:
            for d in listed[2 * g : 2 * g + 2]:
                if d:
                    forward(d)
        now = listed[2 * g - 2 : 2 * g] if 1 <= g <= groups else []
        last = listed[2 * g - 4 : 2 * g - 2] if g >= 2 else []
        for d in now:
            relay(x_move, d)
        for d in last:
            relay(h_move, d)
        if now:
            for d in now:
                settle(x_move, d)
            sources = [flipped(me, d, n) for d in now]
            width = xbuf.shape[3]
            gated = jnp.zeros((2 * cap, gate.shape[1]), F32)
            upped = gated
            for j in range(t):
                x = jnp.concatenate([xbuf[j, s] for s in sources], axis=0)
                part = slice(j * width, (j + 1) * width)
                gated = gated + jnp.dot(x, gate[part, :], preferred_element_type=F32)
                upped = upped + jnp.dot(x, up[part, :], preferred_element_type=F32)
            hidden = (gated / (1.0 + jnp.exp(-gated)) * upped).astype(BF)
            for k in (0, 1):
                hbuf[tp, sources[k]] = hidden[k * cap : (k + 1) * cap]
                h_move(1, now[k]).start()
                h_move(0, now[k]).start()
        if last:
            for d in last:
                settle(h_move, d)
            sources = [flipped(me, d, n) for d in last]
            width = hbuf.shape[3]
            done = jnp.zeros((2 * cap, down.shape[1]), F32)
            for j in range(t):
                h = jnp.concatenate([hbuf[j, s] for s in sources], axis=0)
                done = done + jnp.dot(
                    h, down[j * width : (j + 1) * width, :], preferred_element_type=F32
                )
            done = done.astype(BF)
            for k in (0, 1):
                rbuf[sources[k]] = done[k * cap : (k + 1) * cap]
                if last[k]:
                    give(last[k]).start()
    backbuf[me] = rbuf[me]
    for d in range(1, n):
        give(d).wait_recv()
    flat = jnp.concatenate([backbuf[s] for s in range(n)], axis=0)
    total = stream_keep[...].astype(F32)
    for k in (0, 1):
        total = total + weights[k][:, 0:1] * jnp.dot(
            chosen[k], flat, preferred_element_type=F32
        )
    out[...] = total.astype(BF)
    for d in range(n):
        for kind in (0, 1, 2):
            x_move(kind, d).wait_send()
            h_move(kind, d).wait_send()
        if d:
            send(d).wait_send()
            give(d).wait_send()

    for d in range(1, n):
        dest = lax.rem(me + d, n)

        @pl.when(is_wide(dest))
        def _():
            for part in (0, 1, 2):
                wide(dest, me, d, part).wait_send()

        @pl.when(jnp.logical_not(is_wide(dest)))
        def _():
            for part in (0, 2):
                narrow(dest, me, d, part).wait_send()

        offs(dest, d).wait_send()
        back(dest, d).wait_send()
    pair(0).wait_send()
    pair(1).wait_send()
    far.wait_send()
    for slot, peer in enumerate((partner, across, diagonal)):
        stat(slot, peer).wait_send()


def fast_body(
    queries_one, keys_one, values_one, queries_two, keys_two, values_two, key_offset,
    out_one, out_two, residual, norm_gain, routes, route_weight,
    expert_gate, expert_up, expert_down,
):
    n = lax.axis_size("sp")
    t = lax.axis_size("tp")
    rows, cols = residual.shape
    h1 = queries_one.shape[1] // DH1
    h2 = queries_two.shape[1] // DH2
    cap = 4 * rows // n
    vmem = pl.BlockSpec(memory_space=pltpu.VMEM)
    anyw = pl.BlockSpec(memory_space=pl.ANY)
    dma = pltpu.SemaphoreType.DMA
    large = (
        queries_one, keys_one, values_one, queries_two, keys_two, values_two,
        out_one, out_two, residual, expert_gate[0], expert_up[0], expert_down[0],
    )
    hid = expert_gate.shape[2]
    return pl.pallas_call(
        functools.partial(layer_kernel, n, t, h1, h2, cap),
        out_shape=jax.ShapeDtypeStruct((rows, cols), BF),
        in_specs=[vmem] * 3 + [anyw] * 13,
        out_specs=vmem,
        scratch_shapes=[pltpu.VMEM(a.shape, a.dtype) for a in large]
        + [
            pltpu.VMEM((1, cols), F32),
            pltpu.VMEM((h2, 2, rows, DH1), BF),
            pltpu.VMEM((3, n, rows, DH1), BF),
            pltpu.VMEM((n, 8, rows), F32),
            pltpu.VMEM((n, 8, rows), F32),
            pltpu.VMEM((n, n, rows, DH1), F32),
            pltpu.VMEM((n, n, rows, DH1), F32),
            pltpu.VMEM((n, rows, DH1), BF),
            pltpu.VMEM((n, rows, DH1), BF),
            pltpu.VMEM((2, rows, cols), BF),
            pltpu.VMEM((2, rows, cols), BF),
            pltpu.VMEM((rows, cols), BF),
            pltpu.VMEM((rows, cols), BF),
            pltpu.VMEM((1, 8, rows), F32),
            pltpu.VMEM((3, 8, rows), F32),
            pltpu.VMEM((rows, cols), BF),
            pltpu.VMEM((2, rows, n * cap), BF),
            pltpu.VMEM((2, rows, 128), F32),
            pltpu.VMEM((n, cap, cols), BF),
            pltpu.VMEM((t, n, cap, cols), BF),
            pltpu.VMEM((t, n, cap, hid), BF),
            pltpu.VMEM((n, cap, cols), BF),
            pltpu.VMEM((n, cap, cols), BF),
            dma((13,)),
            dma((n, 3)), dma((n, 3)),
            dma((n,)), dma((n,)),
            dma((n,)), dma((n,)),
            dma((2,)), dma((2,)),
            dma((1,)), dma((1,)),
            dma((3,)), dma((3,)),
            dma((n,)), dma((n,)),
            dma((3, n)), dma((3, n)),
            dma((3, n)), dma((3, n)),
            dma((n,)), dma((n,)),
        ],
        compiler_params=pltpu.CompilerParams(
            collective_id=0, has_side_effects=True, vmem_limit_bytes=60 * 2**20
        ),
        name="layer",
    )(
        key_offset.transpose(1, 2, 0), routes.T, route_weight.T, *large, norm_gain[None, :]
    )


def choose(*arrays):
    heads = arrays[0].shape[1] // DH1 + arrays[3].shape[1] // DH2
    n, t = lax.axis_size("sp"), lax.axis_size("tp")
    fits = heads == n and t == 4 and arrays[0].shape[0] == DH1 and DH1 == 2 * DH2
    fits = fits and arrays[0].shape[1] // DH1 * 2 == n and n % 4 == 0 and n & (n - 1) == 0
    return fast_body(*arrays) if fits else body(*arrays)


def solution(mesh):
    return jax.shard_map(
        choose,
        mesh=mesh,
        in_specs=(
            P("sp", "tp"),
            P("sp", "tp"),
            P("sp", "tp"),
            P("sp", "tp"),
            P("sp", "tp"),
            P("sp", "tp"),
            P("sp", None, "tp"),
            P("tp", None),
            P("tp", None),
            P("sp", "tp"),
            P(),
            P("sp", None),
            P("sp", None),
            P("sp", None, "tp"),
            P("sp", None, "tp"),
            P("sp", None, "tp"),
        ),
        out_specs=P("sp", "tp"),
        check_vma=False,
    )
```

profile of v0, /device:TPU:0, one launch (start us, length us, event | category | flops | bytes accessed | tf_op | source)
XLA Modules:
  0.0 111.4 jit_solution(16702354325943156426)
XLA Ops:
  0.0 109.7 %layer.1 = bf16[128,1024]{1,0:T(8,128)(2,1)} custom-call(bf16[2,4,128]{2,1,0:T(4,128)(2,1)} %bitcast.11, s32[2,128]{1,0:T(2,128)} %bitcast.12, f32[2,128]{1,0:T(2,128)} %bitcast.13, bf16[128,512]{1,0:T(8,128)(2,1)} %q1_hbm.1, bf16[128,512]{1,0:T(8,128)(2,1)} %k1_hbm.1, bf16[128,512]{1,0:T(8,128)(2,1)} %v1_hbm.1, bf16[128,256]{1,0:T(8,128)(2,1)} %q2_hbm.1, ...), custom_call_target="tpu_custom_call" | custom-call | tf_op jit(solution)/shard_map/layer/pallas_call | solution.py:584
  109.7 1.7 %copy.18 = bf16[128,1024]{1,0:T(8,128)(2,1)} copy(bf16[128,1024]{1,0:T(8,128)(2,1)} %layer.1) | data formatting | bytes 524288
where the time goes:
time: 112 us; the launch traced here: 111 us
  Pallas kernels  110 us (98%)
  local copies, waits for them, and re-layouts  1.67 us (1%)
    pallas_call x1, Pallas kernels, fast_body(): pl.pallas_call(functools.partial(layer_kernel, n, t, h1, h2, cap), out_sh...  110 us

commit v1 on v0

--- a/solution.py
+++ b/solution.py
@@ -172,6 +172,15 @@
     return total
 
 
+def folded(block):
+    half = block.shape[0] // 2
+    return jnp.concatenate([block[:half, :DH2], block[half:, :DH2]], axis=1)
+
+
+def unfolded(block):
+    return jnp.concatenate([block[:, :DH2], block[:, DH2:]], axis=0)
+
+
 def turns(n):
     near = list(range(n // 2))
     far = list(range(n - n // 4, n)) + list(range(n // 2, n - n // 4))
@@ -196,7 +205,7 @@
     gate_hbm, up_hbm, down_hbm, gain_hbm,
     out,
     q1_in, k1_in, v1_in, q2_in, k2_in, v2_in, w1_in, w2_in, resid_in, gate_in, up_in, down_in, gain,
-    pk, buf, off, offbuf, carry, acc, obuf, att,
+    pk, pv, buf, off, offbuf, carry, acc, obuf, att,
     pair_out, pair_in, far_out, far_in, stat_out, stat_in, stream_keep, chosen, weights,
     sbuf, xbuf, hbuf, rbuf, backbuf,
     wsem, qs, qr, fs, fr, os_, or_, ps, pr, ys, yr, ss, sr,
@@ -232,8 +241,8 @@
             off[2 * h + (h + g) % 2] = jnp.broadcast_to(off_in[g, h : h + 1, :].astype(F32), (8, rows))
     for h in range(h2):
         lanes = slice(h * DH2, (h + 1) * DH2)
-        pk[h, 0] = jnp.concatenate([q2[:, lanes], k2[:, lanes]], axis=1)
-        pk[h, 1] = jnp.concatenate([v2[:, lanes], jnp.zeros((rows, DH1 - DH2), BF)], axis=1)
+        pk[h] = jnp.concatenate([q2[:, lanes], k2[:, lanes]], axis=1)
+        pv[h] = folded(v2[:, lanes])
     pl.semaphore_wait(barrier, len(peers))
 
     def wide(dest, origin, d, part):
@@ -244,19 +253,20 @@
         )
 
     def narrow(dest, origin, d, part):
-        return pltpu.make_async_remote_copy(
-            pk.at[dest // 2, part // 2],
-            buf.at[part, origin], qs.at[d, part], qr.at[d, part], **to(dest, tp),
-        )
+        if part:
+            src, dst = pv.at[dest // 2], buf.at[2, origin, 0 : rows // 2]
+        else:
+            src, dst = pk.at[dest // 2], buf.at[0, origin]
+        return pltpu.make_async_remote_copy(src, dst, qs.at[d, part], qr.at[d, part], **to(dest, tp))
 
     def offs(dest, d):
         return pltpu.make_async_remote_copy(
             off.at[dest], offbuf.at[me], fs.at[d], fr.at[d], **to(dest, tp)
         )
 
-    order = [d for pair in zip(range(n // 2, n), range(n // 2 - 1, -1, -1)) for d in pair if d]
+    order = [d for pair in zip(range(n // 2, n), range(n // 2)) for d in pair if d]
     for d in order:
-        dest = lax.rem(me + d, n)
+        dest = flipped(me, d, n)
 
         @pl.when(is_wide(dest))
         def _():
@@ -281,8 +291,8 @@
     @pl.when(jnp.logical_not(is_wide(me)))
     def _():
         mine = me // 2
-        buf[0, me] = pk[mine, 0]
-        buf[2, me] = pk[mine, 1]
+        buf[0, me] = pk[mine]
+        buf[2, me, 0 : rows // 2] = pv[mine]
 
     table = jnp.concatenate(
         [routes[...].astype(F32), route_weight[...], jnp.zeros((128 - 4, rows), F32)], axis=0
@@ -307,55 +317,69 @@
     scale = jnp.where(is_wide(me), DH1 ** -0.5, DH2 ** -0.5).astype(F32)
     nt = (((1,), (1,)), ((), ()))
 
-    def block(i, j, own):
-        s = lax.dot_general(buf[0, i], buf[1, j], nt, preferred_element_type=F32)
-        s = s * scale + offbuf[j][0:1, :]
-        soft = jnp.log(1.0 + jnp.exp(-jnp.abs(s)))
-        log_beta = jnp.minimum(s, 0.0) - soft
-        log_rest = log_beta - s
-        if own:
-            r = lax.broadcasted_iota(jnp.int32, s.shape, 0)
-            c = lax.broadcasted_iota(jnp.int32, s.shape, 1)
-            log_rest = jnp.where(c < r, log_rest, 0.0)
-        high = log_rest.astype(BF)
-        low = (log_rest - high.astype(F32)).astype(BF)
-        sums = jnp.dot(high, tri, preferred_element_type=F32) + jnp.dot(
-            low, tri, preferred_element_type=F32
-        )
-        weight = jnp.exp(log_beta + sums[:, :DH1])
-        if own:
-            weight = jnp.where(c < r, weight, 0.0)
-        acc[i, j] = jnp.dot(weight.astype(BF), buf[2, j], preferred_element_type=F32)
-        carry[i, j] = sums[:, DH1:]
+    def blocks(pairs):
+        r = lax.broadcasted_iota(jnp.int32, (rows, rows), 0)
+        c = lax.broadcasted_iota(jnp.int32, (rows, rows), 1)
+        scores = [
+            lax.dot_general(buf[0, i], buf[1, j], nt, preferred_element_type=F32)
+            for i, j, _ in pairs
+        ]
+        betas, highs, lows = [], [], []
+        for (_, j, own), s in zip(pairs, scores):
+            s = s * scale + offbuf[j][0:1, :]
+            soft = jnp.log(1.0 + jnp.exp(-jnp.abs(s)))
+            log_beta = jnp.minimum(s, 0.0) - soft
+            log_rest = log_beta - s
+            if own:
+                log_rest = jnp.where(c < r, log_rest, 0.0)
+            high = log_rest.astype(BF)
+            betas.append(log_beta)
+            highs.append(high)
+            lows.append((log_rest - high.astype(F32)).astype(BF))
+        sums = [
+            jnp.dot(high, tri, preferred_element_type=F32)
+            + jnp.dot(low, tri, preferred_element_type=F32)
+            for high, low in zip(highs, lows)
+        ]
+        weighted = []
+        for (i, j, own), log_beta, total in zip(pairs, betas, sums):
+            weight = jnp.exp(log_beta + total[:, :DH1])
+            if own:
+                weight = jnp.where(c < r, weight, 0.0)
+            weighted.append(weight.astype(BF))
+            carry[i, j] = total[:, DH1:]
+        for (i, j, _), weight in zip(pairs, weighted):
+            acc[i, j] = jnp.dot(weight, buf[2, j], preferred_element_type=F32)
 
     here = []
     for d in [0] + order:
-        source = lax.rem(me + n - d, n)
-        if d:
-            dest = lax.rem(me + d, n)
-
-            @pl.when(is_wide(me))
-            def _():
+        source = flipped(me, d, n)
+
+        @pl.when(is_wide(me))
+        def _():
+            if d:
                 for part in (0, 1, 2):
-                    wide(dest, me, d, part).wait_recv()
-
-            @pl.when(jnp.logical_not(is_wide(me)))
-            def _():
-                for part in (0, 2):
-                    narrow(dest, me, d, part).wait_recv()
-
-            offs(dest, d).wait_recv()
+                    wide(source, me, d, part).wait_recv()
 
         @pl.when(jnp.logical_not(is_wide(me)))
         def _():
+            if d:
+                for part in (0, 2):
+                    narrow(source, me, d, part).wait_recv()
             both = buf[0, source]
             zero = jnp.zeros((rows, DH1 - DH2), BF)
             buf[1, source] = jnp.concatenate([both[:, DH2:], zero], axis=1)
             buf[0, source] = jnp.concatenate([both[:, :DH2], zero], axis=1)
-
-        block(source, source, True)
-        for other in here:
-            block(jnp.maximum(source, other), jnp.minimum(source, other), False)
+            buf[2, source] = jnp.concatenate(
+                [unfolded(buf[2, source, 0 : rows // 2]), zero], axis=1
+            )
+
+        if d:
+            offs(source, d).wait_recv()
+        blocks(
+            [(source, source, True)]
+            + [(jnp.maximum(source, k), jnp.minimum(source, k), False) for k in here]
+        )
         here.append(source)
     for i in range(n):
         total = acc[i, i]
@@ -365,21 +389,53 @@
             passed = passed + carry[i, j]
         obuf[i] = total.astype(BF)
 
-    def back(dest, d):
+    @pl.when(jnp.logical_not(is_wide(me)))
+    def _():
+        for i in range(n):
+            obuf[i, 0 : rows // 2] = folded(obuf[i])
+
+    def back(dest, d, full):
+        part = slice(0, rows if full else rows // 2)
         return pltpu.make_async_remote_copy(
-            obuf.at[dest], att.at[me], os_.at[d], or_.at[d], **to(dest, tp)
-        )
-
+            obuf.at[dest, part], att.at[me, part], os_.at[d], or_.at[d], **to(dest, tp)
+        )
+
+    def each(test, act):
+        for full in (True, False):
+
+            @pl.when(test if full else jnp.logical_not(test))
+            def _():
+                act(full)
+
+    each(
+        is_wide(me),
+        lambda full: [back(flipped(me, d, n), d, full).start() for d in order] and None,
+    )
+    att[me] = obuf[me]
     for d in order:
-        back(lax.rem(me + d, n), d).start()
-    att[me] = obuf[me]
+        dest = flipped(me, d, n)
+
+        @pl.when(is_wide(dest))
+        def _():
+            for part in (0, 1, 2):
+                wide(dest, me, d, part).wait_send()
+
+        @pl.when(jnp.logical_not(is_wide(dest)))
+        def _():
+            for part in (0, 2):
+                narrow(dest, me, d, part).wait_send()
+
+        offs(dest, d).wait_send()
     for load in loads[6:9] + loads[12:]:
         load.wait()
-    for d in range(1, n):
-        back(lax.rem(me + d, n), d).wait_recv()
+    for d in order:
+        dest = flipped(me, d, n)
+        each(is_wide(dest), lambda full: back(dest, d, full).wait_recv())
 
     a1 = jnp.concatenate([att[2 * h + h % 2] for h in range(h1)], axis=1)
-    a2 = jnp.concatenate([att[2 * h + 1 - h % 2][:, :DH2] for h in range(h2)], axis=1)
+    a2 = jnp.concatenate(
+        [unfolded(att[2 * h + 1 - h % 2, 0 : rows // 2]) for h in range(h2)], axis=1
+    )
 
     def partial(target):
         lanes = pl.ds(pl.multiple_of(target * cols, 128), cols)
@@ -399,6 +455,10 @@
     pair(0).wait_recv()
     far_out[...] = (there + pair_in[0].astype(F32)).astype(BF)
     far.start()
+    each(
+        is_wide(me),
+        lambda full: [back(flipped(me, d, n), d, full).wait_send() for d in order] and None,
+    )
     pair_out[1] = partial(partner).astype(BF)
     pair(1).start()
     here = partial(tp)
@@ -540,21 +600,6 @@
             send(d).wait_send()
             give(d).wait_send()
 
-    for d in range(1, n):
-        dest = lax.rem(me + d, n)
-
-        @pl.when(is_wide(dest))
-        def _():
-            for part in (0, 1, 2):
-                wide(dest, me, d, part).wait_send()
-
-        @pl.when(jnp.logical_not(is_wide(dest)))
-        def _():
-            for part in (0, 2):
-                narrow(dest, me, d, part).wait_send()
-
-        offs(dest, d).wait_send()
-        back(dest, d).wait_send()
     pair(0).wait_send()
     pair(1).wait_send()
     far.wait_send()
@@ -583,13 +628,14 @@
     hid = expert_gate.shape[2]
     return pl.pallas_call(
         functools.partial(layer_kernel, n, t, h1, h2, cap),
-        out_shape=jax.ShapeDtypeStruct((rows, cols), BF),
+        out_shape=pltpu.VMEM((rows, cols), BF),
         in_specs=[vmem] * 3 + [anyw] * 13,
         out_specs=vmem,
         scratch_shapes=[pltpu.VMEM(a.shape, a.dtype) for a in large]
         + [
             pltpu.VMEM((1, cols), F32),
-            pltpu.VMEM((h2, 2, rows, DH1), BF),
+            pltpu.VMEM((h2, rows, DH1), BF),
+            pltpu.VMEM((h2, rows // 2, DH1), BF),
             pltpu.VMEM((3, n, rows, DH1), BF),
             pltpu.VMEM((n, 8, rows), F32),
             pltpu.VMEM((n, 8, rows), F32),

time: 112 us -> 102 us (0.911)
  Pallas kernels: 110 us -> 101 us
    pallas_call x1, Pallas kernels: 110 us -> 101 us  [fast_body(): pl.pallas_call(functools.partial(layer_kernel, n, t, h1, h2, cap), out_sh...]
where the time goes in v1:
time: 102 us
  Pallas kernels  101 us (99%)
    pallas_call x1, Pallas kernels, fast_body(): pl.pallas_call(functools.partial(layer_kernel, n, t, h1, h2, cap), out_sh...  101 us

profile of v1, /device:TPU:0, one launch (start us, length us, event | category | flops | bytes accessed | tf_op | source)
XLA Modules:
  0.0 102.1 jit_solution(1246047103510671595)
XLA Ops:
  0.0 101.3 %layer.1 = bf16[128,1024]{1,0:T(8,128)(2,1)S(1)} custom-call(bf16[2,4,128]{2,1,0:T(4,128)(2,1)} %bitcast.11, s32[2,128]{1,0:T(2,128)} %bitcast.12, f32[2,128]{1,0:T(2,128)} %bitcast.13, bf16[128,512]{1,0:T(8,128)(2,1)} %q1_hbm.1, bf16[128,512]{1,0:T(8,128)(2,1)} %k1_hbm.1, bf16[128,512]{1,0:T(8,128)(2,1)} %v1_hbm.1, bf16[128,256]{1,0:T(8,128)(2,1)} %q2_hbm.1, ...), custom_call_target="tpu_custom_call" | custom-call | tf_op jit(solution)/shard_map/layer/pallas_call | solution.py:629
  101.3 0.7 copy.18

commit v2 on v1

--- a/solution.py
+++ b/solution.py
@@ -12,6 +12,8 @@
 
 
 EPS = 1e-06
+PIECES = 4
+PARTS = 2
 
 
 def stick_group(query, keys, values, offset, head_size, own_start, key_block):
@@ -181,15 +183,16 @@
     return jnp.concatenate([block[:, :DH2], block[:, DH2:]], axis=0)
 
 
-def turns(n):
-    near = list(range(n // 2))
-    far = list(range(n - n // 4, n)) + list(range(n // 2, n - n // 4))
-    listed, rest = near[:2], near[2:]
-    for mask in far:
-        listed.append(mask)
-        if rest:
-            listed.append(rest.pop(0))
-    return listed + rest
+SENDS = (
+    ((1, 0), (4, 0), (2, 0)),
+    ((4, 1), (1, 1), (2, 1)),
+    ((5, 0), (5, 1), (3, 0), (3, 1), (6, 0), (6, 1), (7, 0), (7, 1)),
+)
+STEPS = (
+    ("f", 1), ("f", 2), ("s"), ("f", 4), ("r", 0), ("r", 1), ("f", 5), ("r", 2), ("f", 3), ("r", 4),
+    ("x", 4, 1), ("r", 5), ("f", 6), ("x", 5, 2), ("r", 3), ("h", 4, 1), ("f", 7), ("r", 6),
+    ("x", 6, 3), ("h", 5, 2), ("r", 7), ("x", 7, 0), ("h", 6, 3), ("h", 7, 0),
+)
 
 
 def neighbours(tp, t):
@@ -204,11 +207,12 @@
     q1_hbm, k1_hbm, v1_hbm, q2_hbm, k2_hbm, v2_hbm, w1_hbm, w2_hbm, resid_hbm,
     gate_hbm, up_hbm, down_hbm, gain_hbm,
     out,
-    q1_in, k1_in, v1_in, q2_in, k2_in, v2_in, w1_in, w2_in, resid_in, gate_in, up_in, down_in, gain,
+    q1_in, k1_in, v1_in, q2_in, k2_in, v2_in, w_in, resid_in, gate_in, up_in, down_in, gain,
     pk, pv, buf, off, offbuf, carry, acc, obuf, att,
-    pair_out, pair_in, far_out, far_in, stat_out, stat_in, stream_keep, chosen, weights,
+    pair_out, pair_in, far_out, far_in, mine, stat_out, stat_in, fac_out, fac_in,
+    stream_keep, scaled, chosen, picker, weights,
     sbuf, xbuf, hbuf, rbuf, backbuf,
-    wsem, qs, qr, fs, fr, os_, or_, ps, pr, ys, yr, ss, sr,
+    wsem, qs, qr, fs, fr, os_, or_, ps, pr, ys, yr, ss, sr, cs, cr,
     ds_, dr, xs, xr, hs, hr, rs, rr,
 ):
     in_hbm = (
@@ -216,8 +220,8 @@
         gate_hbm, up_hbm, down_hbm,
     )
     in_vmem = (
-        q1_in, k1_in, v1_in, q2_in, k2_in, v2_in, w1_in, w2_in, resid_in,
-        gate_in, up_in, down_in,
+        q1_in, k1_in, v1_in, q2_in, k2_in, v2_in,
+        w_in.at[0 : h1 * DH1], w_in.at[h1 * DH1 :], resid_in, gate_in, up_in, down_in,
     )
     me = lax.axis_index("sp")
     tp = lax.axis_index("tp")
@@ -233,7 +237,8 @@
     loads = [pltpu.make_async_copy(a, b, wsem.at[i]) for i, (a, b) in enumerate(pairs)]
     for load in loads:
         load.start()
-    q1, k1, v1, q2, k2, v2, w1, w2, resid_, gate, up, down = in_vmem
+    q1, k1, v1, q2, k2, v2 = in_vmem[:6]
+    gate, up, down = in_vmem[9:]
     for load in loads[:6]:
         load.wait()
     for g in range(2):
@@ -310,6 +315,7 @@
         )
         chosen[k] = jnp.where(slots == slot, 1.0, 0.0).astype(BF)
         weights[k] = jnp.broadcast_to(table[:, 2 + k : 3 + k], (rows, 128))
+    picker[...] = (chosen[0] + chosen[1]).astype(F32).T.astype(BF)
 
     lane = lax.broadcasted_iota(jnp.int32, (DH1, 2 * DH1), 1)
     row = lax.broadcasted_iota(jnp.int32, (DH1, 2 * DH1), 0)
@@ -437,76 +443,126 @@
         [unfolded(att[2 * h + 1 - h % 2, 0 : rows // 2]) for h in range(h2)], axis=1
     )
 
-    def partial(target):
-        lanes = pl.ds(pl.multiple_of(target * cols, 128), cols)
-        return jnp.dot(a1, w1[:, lanes], preferred_element_type=F32) + jnp.dot(
-            a2, w2[:, lanes], preferred_element_type=F32
-        )
-
-    def pair(slot):
-        return pltpu.make_async_remote_copy(
-            pair_out.at[slot], pair_in.at[slot], ps.at[slot], pr.at[slot], **to(me, partner)
-        )
-
-    far = pltpu.make_async_remote_copy(far_out, far_in, ys.at[0], yr.at[0], **to(me, across))
-    pair_out[0] = partial(diagonal).astype(BF)
-    pair(0).start()
-    there = partial(across)
-    pair(0).wait_recv()
-    far_out[...] = (there + pair_in[0].astype(F32)).astype(BF)
-    far.start()
+    a = jnp.concatenate([a1, a2], axis=1)
+    pieces, _, width = mine.shape
+
+    def partial(target, c):
+        lanes = pl.ds(pl.multiple_of(target * cols + c * width, 128), width)
+        return jnp.dot(a, w_in[:, lanes], preferred_element_type=F32)
+
+    def pair(slot, c):
+        return pltpu.make_async_remote_copy(
+            pair_out.at[slot, c], pair_in.at[slot, c], ps.at[slot, c], pr.at[slot, c],
+            **to(me, partner),
+        )
+
+    def far(c):
+        return pltpu.make_async_remote_copy(
+            far_out.at[c], far_in.at[c], ys.at[c], yr.at[c], **to(me, across)
+        )
+
+    for c in range(pieces):
+        pair_out[0, c] = partial(diagonal, c).astype(BF)
+        pair(0, c).start()
+    for c in range(pieces):
+        there = partial(across, c)
+        pair(0, c).wait_recv()
+        far_out[c] = (there + pair_in[0, c].astype(F32)).astype(BF)
+        far(c).start()
+    for c in range(pieces):
+        pair_out[1, c] = partial(partner, c).astype(BF)
+        pair(1, c).start()
     each(
         is_wide(me),
         lambda full: [back(flipped(me, d, n), d, full).wait_send() for d in order] and None,
     )
-    pair_out[1] = partial(partner).astype(BF)
-    pair(1).start()
-    here = partial(tp)
-    pair(1).wait_recv()
-    here = here + pair_in[1].astype(F32)
-    far.wait_recv()
-    stream = (resid_[...].astype(F32) + (here + far_in[...].astype(F32))).astype(BF)
-    stream_keep[...] = stream
-    stream = stream.astype(F32)
-    squares = jnp.sum(stream * stream, axis=1, keepdims=True)
-    stat_out[0] = jnp.broadcast_to(squares, (rows, 128)).T[0:8, :]
+    for c in range(pieces):
+        own = partial(tp, c)
+        pair(1, c).wait_recv()
+        mine[c] = own + pair_in[1, c].astype(F32)
+    parts, _, _, wide_part = sbuf.shape
+    per = pieces // parts
 
     def stat(slot, peer):
         return pltpu.make_async_remote_copy(
             stat_out.at[0], stat_in.at[slot], ss.at[slot], sr.at[slot], **to(me, peer)
         )
 
-    for slot, peer in enumerate((partner, across, diagonal)):
-        stat(slot, peer).start()
-    for slot, peer in enumerate((partner, across, diagonal)):
-        stat(slot, peer).wait_recv()
-    total = stat_out[0] + stat_in[0] + stat_in[1] + stat_in[2]
-    total = jnp.broadcast_to(total[0:1, :], (128, rows)).T[:, 0:1]
-    normed = (stream * lax.rsqrt(total / (t * cols) + EPS) * gain[...]).astype(BF)
-
-    outgoing = lax.dot_general(
-        chosen[0] + chosen[1], normed, (((0,), (0,)), ((), ())), preferred_element_type=F32
-    ).astype(BF)
-    for s in range(n):
-        sbuf[s] = outgoing[s * cap : (s + 1) * cap]
-
-    def send(d):
+    def send(d, p):
         dest = flipped(me, d, n)
         return pltpu.make_async_remote_copy(
-            sbuf.at[dest], xbuf.at[tp, me], ds_.at[d], dr.at[d], **to(dest, tp)
-        )
-
-    def spread(ref, sends, recvs, kind, d):
+            sbuf.at[p, dest], xbuf.at[tp, p, me], ds_.at[d, p], dr.at[d, p], **to(dest, tp)
+        )
+
+    def x_move(kind, d, p):
         s = flipped(me, d, n)
         share = across if kind == 2 else tp
         peer = across if kind == 1 else partner
         return pltpu.make_async_remote_copy(
-            ref.at[share, s], ref.at[share, s], sends.at[kind, d], recvs.at[kind, d],
+            xbuf.at[share, p, s], xbuf.at[share, p, s], xs.at[kind, d, p], xr.at[kind, d, p],
             **to(me, peer),
         )
 
-    x_move = functools.partial(spread, xbuf, xs, xr)
-    h_move = functools.partial(spread, hbuf, hs, hr)
+    def h_move(kind, d):
+        s = flipped(me, d, n)
+        share = across if kind == 2 else tp
+        peer = across if kind == 1 else partner
+        return pltpu.make_async_remote_copy(
+            hbuf.at[share, s], hbuf.at[share, s], hs.at[kind, d], hr.at[kind, d],
+            **to(me, peer),
+        )
+
+    def factor(d):
+        dest = flipped(me, d, n)
+        return pltpu.make_async_remote_copy(
+            fac_out.at[dest], fac_in.at[me], cs.at[d], cr.at[d], **to(dest, tp)
+        )
+
+    peers = tuple(enumerate((partner, across, diagonal)))
+    squares = jnp.zeros((rows, 1), F32)
+    for c in range(pieces):
+        lanes = slice(c * width, (c + 1) * width)
+        far(c).wait_recv()
+        stream = (resid_in[:, lanes].astype(F32) + (mine[c] + far_in[c].astype(F32))).astype(BF)
+        stream_keep[:, lanes] = stream
+        stream = stream.astype(F32)
+        scaled[:, lanes] = (stream * gain[:, lanes]).astype(BF)
+        squares = squares + jnp.sum(stream * stream, axis=1, keepdims=True)
+        if c == pieces - 1:
+            stat_out[0] = jnp.broadcast_to(squares, (rows, 128)).T[0:8, :]
+            for slot, peer in peers:
+                stat(slot, peer).start()
+        if (c + 1) % per == 0:
+            p = c // per
+            part = slice(p * wide_part, (p + 1) * wide_part)
+            outgoing = jnp.dot(
+                picker[...], scaled[:, part], preferred_element_type=F32
+            ).astype(BF)
+            for s in range(n):
+                sbuf[p, s] = outgoing[s * cap : (s + 1) * cap]
+            for d, q in SENDS[p]:
+                send(d, q).start()
+            xbuf[tp, p, me] = sbuf[p, me]
+            x_move(1, 0, p).start()
+            x_move(0, 0, p).start()
+    def norms():
+        for slot, peer in peers:
+            stat(slot, peer).wait_recv()
+        total = stat_out[0] + stat_in[0] + stat_in[1] + stat_in[2]
+        total = jnp.broadcast_to(total[0:1, :], (128, rows)).T[:, 0:1]
+        inverse = lax.rsqrt(total / (t * cols) + EPS)
+        inverse = jnp.sum(
+            (chosen[0] + chosen[1]).astype(F32) * inverse, axis=0, keepdims=True
+        )
+        for s in range(n):
+            spot = inverse[:, s * cap : (s + 1) * cap]
+            spot = jnp.concatenate([spot, jnp.zeros((1, 128 - cap), F32)], axis=1)
+            fac_out[s] = jnp.broadcast_to(spot, (8, 128))
+        for d in order:
+            factor(d).start()
+        fac_in[me] = fac_out[me]
+        for d, q in SENDS[-1]:
+            send(d, q).start()
 
     def give(d):
         dest = flipped(me, d, n)
@@ -514,74 +570,94 @@
             rbuf.at[dest], backbuf.at[me], rs.at[d], rr.at[d], **to(dest, tp)
         )
 
-    listed = turns(n)
-    for d in listed[1:]:
-        send(d).start()
-    xbuf[tp, me] = sbuf[me]
-    x_move(1, 0).start()
-    x_move(0, 0).start()
     for load in loads[9:12]:
         load.wait()
 
-    def forward(d):
-        send(d).wait_recv()
-        x_move(1, d).start()
-        x_move(0, d).start()
-
-    def relay(move, d):
-        move(1, d).wait_recv()
-        move(2, d).start()
-
-    def settle(move, d):
-        move(0, d).wait_recv()
-        move(2, d).wait_recv()
-
-    groups = n // 2
-
-    for g in range(groups + 2):
-        if g < groups:
-            for d in listed[2 * g : 2 * g + 2]:
-                if d:
-                    forward(d)
-        now = listed[2 * g - 2 : 2 * g] if 1 <= g <= groups else []
-        last = listed[2 * g - 4 : 2 * g - 2] if g >= 2 else []
-        for d in now:
-            relay(x_move, d)
-        for d in last:
-            relay(h_move, d)
-        if now:
-            for d in now:
-                settle(x_move, d)
-            sources = [flipped(me, d, n) for d in now]
-            width = xbuf.shape[3]
-            gated = jnp.zeros((2 * cap, gate.shape[1]), F32)
-            upped = gated
-            for j in range(t):
-                x = jnp.concatenate([xbuf[j, s] for s in sources], axis=0)
-                part = slice(j * width, (j + 1) * width)
-                gated = gated + jnp.dot(x, gate[part, :], preferred_element_type=F32)
-                upped = upped + jnp.dot(x, up[part, :], preferred_element_type=F32)
-            hidden = (gated / (1.0 + jnp.exp(-gated)) * upped).astype(BF)
-            for k in (0, 1):
-                hbuf[tp, sources[k]] = hidden[k * cap : (k + 1) * cap]
-                h_move(1, now[k]).start()
-                h_move(0, now[k]).start()
-        if last:
-            for d in last:
-                settle(h_move, d)
-            sources = [flipped(me, d, n) for d in last]
-            width = hbuf.shape[3]
-            done = jnp.zeros((2 * cap, down.shape[1]), F32)
-            for j in range(t):
-                h = jnp.concatenate([hbuf[j, s] for s in sources], axis=0)
-                done = done + jnp.dot(
-                    h, down[j * width : (j + 1) * width, :], preferred_element_type=F32
+    def relay(move):
+        move(1).wait_recv()
+        move(2).start()
+
+    def settle(move):
+        move(0).wait_recv()
+        move(2).wait_recv()
+
+    def enter(members):
+        for d in members:
+            if d:
+                factor(d).wait_recv()
+            for p in range(parts):
+                settle(lambda kind: x_move(kind, d, p))
+        sources = [flipped(me, d, n) for d in members]
+        column = jnp.concatenate([fac_in[s][0:1, :cap] for s in sources], axis=1)
+        column = jnp.broadcast_to(column, (128, len(members) * cap)).T[:, 0:1]
+        gated = jnp.zeros((len(members) * cap, gate.shape[1]), F32)
+        upped = gated
+        for j in range(t):
+            for p in range(parts):
+                x = jnp.concatenate([xbuf[j, p, s] for s in sources], axis=0)
+                first = j * cols + p * wide_part
+                gated = gated + jnp.dot(
+                    x, gate[first : first + wide_part, :], preferred_element_type=F32
                 )
-            done = done.astype(BF)
-            for k in (0, 1):
-                rbuf[sources[k]] = done[k * cap : (k + 1) * cap]
-                if last[k]:
-                    give(last[k]).start()
+                upped = upped + jnp.dot(
+                    x, up[first : first + wide_part, :], preferred_element_type=F32
+                )
+        gated = gated * column
+        hidden = (gated / (1.0 + jnp.exp(-gated)) * (upped * column)).astype(BF)
+        for k, d in enumerate(members):
+            hbuf[tp, sources[k]] = hidden[k * cap : (k + 1) * cap]
+            h_move(1, d).start()
+            h_move(0, d).start()
+
+    def leave(members):
+        for d in members:
+            relay(lambda kind: h_move(kind, d))
+        for d in members:
+            settle(lambda kind: h_move(kind, d))
+        sources = [flipped(me, d, n) for d in members]
+        size = hbuf.shape[3]
+        done = jnp.zeros((len(members) * cap, down.shape[1]), F32)
+        for j in range(t):
+            h = jnp.concatenate([hbuf[j, s] for s in sources], axis=0)
+            done = done + jnp.dot(
+                h, down[j * size : (j + 1) * size, :], preferred_element_type=F32
+            )
+        done = done.astype(BF)
+        for k, d in enumerate(members):
+            rbuf[sources[k]] = done[k * cap : (k + 1) * cap]
+            if d:
+                give(d).start()
+
+    for kind, *members in STEPS:
+        if kind == "s":
+            norms()
+        elif kind == "f":
+            for p in range(parts):
+                send(members[0], p).wait_recv()
+                x_move(1, members[0], p).start()
+                x_move(0, members[0], p).start()
+        elif kind == "r":
+            for p in range(parts):
+                relay(lambda k: x_move(k, members[0], p))
+        elif kind == "x":
+            enter(members)
+        else:
+            if (kind, *members) == STEPS[-1]:
+                for d in range(n):
+                    for p in range(parts):
+                        for k in (0, 1, 2):
+                            x_move(k, d, p).wait_send()
+                        if d:
+                            send(d, p).wait_send()
+                    if d:
+                        factor(d).wait_send()
+                for c in range(pieces):
+                    pair(0, c).wait_send()
+                    pair(1, c).wait_send()
+                    far(c).wait_send()
+                for slot, peer in peers:
+                    stat(slot, peer).wait_send()
+            leave(members)
     backbuf[me] = rbuf[me]
     for d in range(1, n):
         give(d).wait_recv()
@@ -594,17 +670,9 @@
     out[...] = total.astype(BF)
     for d in range(n):
         for kind in (0, 1, 2):
-            x_move(kind, d).wait_send()
             h_move(kind, d).wait_send()
         if d:
-            send(d).wait_send()
             give(d).wait_send()
-
-    pair(0).wait_send()
-    pair(1).wait_send()
-    far.wait_send()
-    for slot, peer in enumerate((partner, across, diagonal)):
-        stat(slot, peer).wait_send()
 
 
 def fast_body(
@@ -631,7 +699,9 @@
         out_shape=pltpu.VMEM((rows, cols), BF),
         in_specs=[vmem] * 3 + [anyw] * 13,
         out_specs=vmem,
-        scratch_shapes=[pltpu.VMEM(a.shape, a.dtype) for a in large]
+        scratch_shapes=[pltpu.VMEM(a.shape, a.dtype) for a in large[:6]]
+        + [pltpu.VMEM((out_one.shape[0] + out_two.shape[0], out_one.shape[1]), BF)]
+        + [pltpu.VMEM(a.shape, a.dtype) for a in large[8:]]
         + [
             pltpu.VMEM((1, cols), F32),
             pltpu.VMEM((h2, rows, DH1), BF),
@@ -643,17 +713,22 @@
             pltpu.VMEM((n, n, rows, DH1), F32),
             pltpu.VMEM((n, rows, DH1), BF),
             pltpu.VMEM((n, rows, DH1), BF),
-            pltpu.VMEM((2, rows, cols), BF),
-            pltpu.VMEM((2, rows, cols), BF),
+            pltpu.VMEM((2, PIECES, rows, cols // PIECES), BF),
+            pltpu.VMEM((2, PIECES, rows, cols // PIECES), BF),
+            pltpu.VMEM((PIECES, rows, cols // PIECES), BF),
+            pltpu.VMEM((PIECES, rows, cols // PIECES), BF),
+            pltpu.VMEM((PIECES, rows, cols // PIECES), F32),
+            pltpu.VMEM((1, 8, rows), F32),
+            pltpu.VMEM((3, 8, rows), F32),
+            pltpu.VMEM((n, 8, 128), F32),
+            pltpu.VMEM((n, 8, 128), F32),
             pltpu.VMEM((rows, cols), BF),
             pltpu.VMEM((rows, cols), BF),
-            pltpu.VMEM((1, 8, rows), F32),
-            pltpu.VMEM((3, 8, rows), F32),
-            pltpu.VMEM((rows, cols), BF),
             pltpu.VMEM((2, rows, n * cap), BF),
+            pltpu.VMEM((n * cap, rows), BF),
             pltpu.VMEM((2, rows, 128), F32),
-            pltpu.VMEM((n, cap, cols), BF),
-            pltpu.VMEM((t, n, cap, cols), BF),
+            pltpu.VMEM((PARTS, n, cap, cols // PARTS), BF),
+            pltpu.VMEM((t, PARTS, n, cap, cols // PARTS), BF),
             pltpu.VMEM((t, n, cap, hid), BF),
             pltpu.VMEM((n, cap, cols), BF),
             pltpu.VMEM((n, cap, cols), BF),
@@ -661,11 +736,12 @@
             dma((n, 3)), dma((n, 3)),
             dma((n,)), dma((n,)),
             dma((n,)), dma((n,)),
-            dma((2,)), dma((2,)),
-            dma((1,)), dma((1,)),
+            dma((2, PIECES)), dma((2, PIECES)),
+            dma((PIECES,)), dma((PIECES,)),
             dma((3,)), dma((3,)),
             dma((n,)), dma((n,)),
-            dma((3, n)), dma((3, n)),
+            dma((n, PARTS)), dma((n, PARTS)),
+            dma((3, n, PARTS)), dma((3, n, PARTS)),
             dma((3, n)), dma((3, n)),
             dma((n,)), dma((n,)),
         ],
@@ -682,7 +758,7 @@
     heads = arrays[0].shape[1] // DH1 + arrays[3].shape[1] // DH2
     n, t = lax.axis_size("sp"), lax.axis_size("tp")
     fits = heads == n and t == 4 and arrays[0].shape[0] == DH1 and DH1 == 2 * DH2
-    fits = fits and arrays[0].shape[1] // DH1 * 2 == n and n % 4 == 0 and n & (n - 1) == 0
+    fits = fits and arrays[0].shape[1] // DH1 * 2 == n and n == 8 and DH1 * 4 // n * 2 == 128
     return fast_body(*arrays) if fits else body(*arrays)
 
 

time: 102 us -> 94.4 us (0.925); the launches traced: 102 us -> 92.9 us
  Pallas kernels: 101 us -> 92.2 us
    pallas_call x1, Pallas kernels: 101 us -> 92.2 us  [fast_body(): pl.pallas_call(functools.partial(layer_kernel, n, t, h1, h2, cap), out_sh...]
where the time goes in v2:
time: 94.4 us; the launch traced here: 92.9 us
  Pallas kernels  92.2 us (98%)
    pallas_call x1, Pallas kernels, fast_body(): pl.pallas_call(functools.partial(layer_kernel, n, t, h1, h2, cap), out_sh...  92.2 us

profile of v2, /device:TPU:0, one launch (start us, length us, event | category | flops | bytes accessed | tf_op | source)
XLA Modules:
  0.0 92.9 jit_solution(14409672286772855025)
XLA Ops:
  0.0 92.2 %layer.1 = bf16[128,1024]{1,0:T(8,128)(2,1)S(1)} custom-call(bf16[2,4,128]{2,1,0:T(4,128)(2,1)} %bitcast.11, s32[2,128]{1,0:T(2,128)} %bitcast.12, f32[2,128]{1,0:T(2,128)} %bitcast.13, bf16[128,512]{1,0:T(8,128)(2,1)} %q1_hbm.1, bf16[128,512]{1,0:T(8,128)(2,1)} %k1_hbm.1, bf16[128,512]{1,0:T(8,128)(2,1)} %v1_hbm.1, bf16[128,256]{1,0:T(8,128)(2,1)} %q2_hbm.1, ...), custom_call_target="tpu_custom_call" | custom-call | tf_op jit(solution)/shard_map/layer/pallas_call | solution.py:697
  92.2 0.7 copy.18

commit v3 on v2

--- a/solution.py
+++ b/solution.py
@@ -184,14 +184,15 @@
 
 
 SENDS = (
-    ((1, 0), (4, 0), (2, 0)),
-    ((4, 1), (1, 1), (2, 1)),
-    ((5, 0), (5, 1), (3, 0), (3, 1), (6, 0), (6, 1), (7, 0), (7, 1)),
+    ((1, 0), (4, 0)),
+    ((4, 1), (1, 1), (2, 0), (2, 1), (5, 0)),
+    ((5, 1), (3, 0), (3, 1), (6, 0), (6, 1), (7, 0), (7, 1)),
 )
 STEPS = (
-    ("f", 1), ("f", 2), ("s"), ("f", 4), ("r", 0), ("r", 1), ("f", 5), ("r", 2), ("f", 3), ("r", 4),
-    ("x", 4, 1), ("r", 5), ("f", 6), ("x", 5, 2), ("r", 3), ("h", 4, 1), ("f", 7), ("r", 6),
-    ("x", 6, 3), ("h", 5, 2), ("r", 7), ("x", 7, 0), ("h", 6, 3), ("h", 7, 0),
+    ("f", 1), ("f", 4), ("s"), ("f", 2), ("r", 0), ("r", 1), ("r", 4), ("f", 5), ("x", 4, 1),
+    ("r", 2), ("f", 3), ("r", 5), ("x", 5, 2), ("f", 6), ("q", 4), ("q", 1), ("r", 3), ("h", 4, 1),
+    ("f", 7), ("q", 5), ("q", 2), ("h", 5, 2), ("r", 6), ("x", 6, 3), ("r", 7), ("x", 7, 0), ("q", 6),
+    ("q", 3), ("h", 6, 3), ("q", 7), ("q", 0), ("h", 7, 0),
 )
 
 
@@ -611,8 +612,6 @@
 
     def leave(members):
         for d in members:
-            relay(lambda kind: h_move(kind, d))
-        for d in members:
             settle(lambda kind: h_move(kind, d))
         sources = [flipped(me, d, n) for d in members]
         size = hbuf.shape[3]
@@ -641,6 +640,8 @@
                 relay(lambda k: x_move(k, members[0], p))
         elif kind == "x":
             enter(members)
+        elif kind == "q":
+            relay(lambda k: h_move(k, members[0]))
         else:
             if (kind, *members) == STEPS[-1]:
                 for d in range(n):

time: 94.4 us -> 90.3 us (0.957); the launches traced: 92.9 us -> 90 us
  Pallas kernels: 92.2 us -> 89.3 us
    pallas_call x1, Pallas kernels: 92.2 us -> 89.3 us  [fast_body(): pl.pallas_call(functools.partial(layer_kernel, n, t, h1, h2, cap), out_sh...]
where the time goes in v3:
time: 90.3 us; the launch traced here: 90 us
  Pallas kernels  89.3 us (99%)
    pallas_call x1, Pallas kernels, fast_body(): pl.pallas_call(functools.partial(layer_kernel, n, t, h1, h2, cap), out_sh...  89.3 us

profile of v3, /device:TPU:0, one launch (start us, length us, event | category | flops | bytes accessed | tf_op | source)
XLA Modules:
  0.0 90.0 jit_solution(4234152256948704682)
XLA Ops:
  0.0 89.3 %layer.1 = bf16[128,1024]{1,0:T(8,128)(2,1)S(1)} custom-call(bf16[2,4,128]{2,1,0:T(4,128)(2,1)} %bitcast.11, s32[2,128]{1,0:T(2,128)} %bitcast.12, f32[2,128]{1,0:T(2,128)} %bitcast.13, bf16[128,512]{1,0:T(8,128)(2,1)} %q1_hbm.1, bf16[128,512]{1,0:T(8,128)(2,1)} %k1_hbm.1, bf16[128,512]{1,0:T(8,128)(2,1)} %v1_hbm.1, bf16[128,256]{1,0:T(8,128)(2,1)} %q2_hbm.1, ...), custom_call_target="tpu_custom_call" | custom-call | tf_op jit(solution)/shard_map/layer/pallas_call | solution.py:698
  89.3 0.7 copy.18

commit v4 on v3

--- a/solution.py
+++ b/solution.py
@@ -660,14 +660,18 @@
                     stat(slot, peer).wait_send()
             leave(members)
     backbuf[me] = rbuf[me]
-    for d in range(1, n):
-        give(d).wait_recv()
-    flat = jnp.concatenate([backbuf[s] for s in range(n)], axis=0)
     total = stream_keep[...].astype(F32)
-    for k in (0, 1):
-        total = total + weights[k][:, 0:1] * jnp.dot(
-            chosen[k], flat, preferred_element_type=F32
-        )
+    for first in (4, 2, 0, 6):
+        for d in (first, first + 1):
+            if d:
+                give(d).wait_recv()
+        base = flipped(me, first, n) // 2
+        lanes = pl.ds(pl.multiple_of(base * 2 * cap, 2 * cap), 2 * cap)
+        both = jnp.concatenate([backbuf[2 * base], backbuf[2 * base + 1]], axis=0)
+        for k in (0, 1):
+            total = total + weights[k][:, 0:1] * jnp.dot(
+                chosen[k, :, lanes], both, preferred_element_type=F32
+            )
     out[...] = total.astype(BF)
     for d in range(n):
         for kind in (0, 1, 2):

time: 90.3 us -> 90.1 us (level)
  no operation moved by 1% of the time
where the time goes in v4:
time: 90.1 us; the launch traced here: 89.8 us
  Pallas kernels  89.1 us (99%)
    pallas_call x1, Pallas kernels, fast_body(): pl.pallas_call(functools.partial(layer_kernel, n, t, h1, h2, cap), out_sh...  89.1 us

profile of v4, /device:TPU:0, one launch (start us, length us, event | category | flops | bytes accessed | tf_op | source)
XLA Modules:
  0.0 89.8 jit_solution(17102560819061059304)
XLA Ops:
  0.0 89.1 %layer.1 = bf16[128,1024]{1,0:T(8,128)(2,1)S(1)} custom-call(bf16[2,4,128]{2,1,0:T(4,128)(2,1)} %bitcast.11, s32[2,128]{1,0:T(2,128)} %bitcast.12, f32[2,128]{1,0:T(2,128)} %bitcast.13, bf16[128,512]{1,0:T(8,128)(2,1)} %q1_hbm.1, bf16[128,512]{1,0:T(8,128)(2,1)} %k1_hbm.1, bf16[128,512]{1,0:T(8,128)(2,1)} %v1_hbm.1, bf16[128,256]{1,0:T(8,128)(2,1)} %q2_hbm.1, ...), custom_call_target="tpu_custom_call" | custom-call | tf_op jit(solution)/shard_map/layer/pallas_call | solution.py:702
  89.1 0.7 copy.18
